TPU v7x, 512 devices: a whole 4x8x8 slice. The times are simulated.
512 devices in a mesh: sp: 32 (over z, x), tp: 16 (over y, core).
Axes of the slice: x: 4, y: 8, z: 8, core: 2. Of those that a mesh axis runs over, the one named last changes fastest.
Arguments:
- queries: bfloat16 [8192, 1024], P('sp', 'tp'), may hold values from -64 to 64
- keys: bfloat16 [8192, 1024], P('sp', 'tp'), may hold values from -64 to 64
- values: bfloat16 [8192, 1024], P('sp', 'tp'), may hold values from -6 to 6
- cum_gate: float32 [16, 8192], P('tp'), may hold values from -8192 to 0, as said below
- out_weight: bfloat16 [1024, 2048], P('tp'), may hold values from -0.375 to 0.375
- resid: bfloat16 [8192, 2048], P('sp'), may hold values from -6 to 6
- norm_gain: float32 [2048], replicated, may hold values from 0.1 to 1.9
- routes: int32 [8192, 2], P('sp'), may hold values from 0 to 31, all different within a row; in each aligned block of 256 rows (0 to 255, 256 to 511, ...) at most 20 rows name the same one
- route_weight: float32 [8192, 2], P('sp'), may hold values from 0.1 to 0.9
- gate_weight: bfloat16 [32, 2048, 4096], P('sp', None, 'tp'), may hold values from -0.125 to 0.125
- up_weight: bfloat16 [32, 2048, 4096], P('sp', None, 'tp'), may hold values from -0.125 to 0.125
- down_weight: bfloat16 [32, 4096, 2048], P('sp', 'tp'), may hold values from -0.09375 to 0.09375
Outputs:
- layer_out: bfloat16 [8192, 2048], P('sp', 'tp')
Inputs may be any that keep to these rules, and one draw needn't show every extreme that they name: `routes`: each token names 2 different experts. Among the rows of one index of sp, no expert is named more than 20 times, a bound that some block reaches. `cum_gate`: each head's row does not rise along the positions.
All inputs are finite; a program needn't handle non-finite values.
Results may differ from a plain program's by a relative error of at most 0.015.
Values may be sent and summed in bfloat16 or wider, within the bound.
No kernel may reach another device: no remote copies, remote signals or barrier semaphores. Data moves between devices by JAX's collectives and lax.ppermute only.
A program may use at most 64 MiB of HBM per device.

v0:
```python
import math
import jax
import jax.numpy as jnp
from jax import lax
from jax.sharding import PartitionSpec as P

HD = 64
epsilon = 1e-06


def in_one_piece(arrays, axis, dim, along):
    ends, at = ([], 0)
    for a in arrays[:-1]:
        at += a.shape[along]
        ends.append(at)
    both = jnp.concatenate(arrays, axis=along)
    return tuple(jnp.split(lax.all_gather(both, axis, axis=dim, tiled=True), ends, axis=along))


def in_blocks(x, dim, length):
    before, after = (x.shape[:dim], x.shape[dim + 1 :])
    return jnp.moveaxis(x.reshape(*before, length, -1, *after), dim, 0)


def sum_at_owner(x, axis, dim):
    tiles = in_blocks(x, dim, lax.axis_size(axis))
    arrived = lax.all_to_all(tiles, axis, split_axis=0, concat_axis=0, tiled=True)
    return arrived.astype(jnp.float32).sum(axis=0)


def from_everyone(x, axis):
    length = lax.axis_size(axis)
    return lax.all_to_all(jnp.broadcast_to(x[None], (length, *x.shape)), axis, 0, 0, tiled=True)


def of_everyone(x, axis):
    everything = from_everyone(x, axis)
    return jnp.sum(everything, axis=0)


def attend_block(
    carried, query_heads, cum_query, key_rows, value_rows, cum_keys, query_first, key_first
):
    best_score, weight_sum, value_sum = carried
    score_scale = query_heads.shape[-1] ** (-0.5)
    scores = (
        jnp.einsum("hqd,hkd->hqk", query_heads, key_rows, preferred_element_type=jnp.float32)
        * score_scale
    )
    scores = scores + cum_query[:, :, None] - cum_keys[:, None, :]
    query_pos = query_first + jnp.arange(query_heads.shape[1], dtype=jnp.int32)
    key_pos = key_first + jnp.arange(key_rows.shape[1], dtype=jnp.int32)
    permitted_mask = (key_pos[None, :] <= query_pos[:, None])[None]
    new_best = jnp.maximum(
        best_score, jnp.max(jnp.where(permitted_mask, scores, -jnp.inf), axis=-1)
    )
    weights = jnp.where(permitted_mask, jnp.exp(scores - new_best[..., None]), 0.0)
    shrink = jnp.exp(best_score - new_best)
    weight_sum = weight_sum * shrink + jnp.sum(weights, axis=-1)
    value_sum = value_sum * shrink[..., None] + jnp.einsum(
        "hqk,hkd->hqd", weights.astype(jnp.bfloat16), value_rows, preferred_element_type=jnp.float32
    )
    return (new_best, weight_sum, value_sum)


def local(
    queries,
    keys,
    values,
    cum_gate,
    out_weight,
    resid,
    norm_gain,
    routes,
    route_weight,
    gate_weight,
    up_weight,
    down_weight,
):
    rows_here = queries.shape[0]
    heads_here = queries.shape[1] // HD
    sp_count = lax.axis_size("sp")
    tp_count = lax.axis_size("tp")
    shift_amount = lax.axis_index("sp") * rows_here
    model_width = resid.shape[1]
    columns = model_width // tp_count
    column_first = lax.axis_index("tp") * columns
    query_heads = queries.reshape(rows_here, heads_here, HD).transpose(1, 0, 2)
    cum_query = lax.dynamic_slice_in_dim(cum_gate, shift_amount, rows_here, 1)
    start_state = (
        jnp.full((heads_here, rows_here), -1e30, jnp.float32),
        jnp.zeros((heads_here, rows_here), jnp.float32),
        jnp.zeros((heads_here, rows_here, HD), jnp.float32),
    )
    key_part, value_part = in_one_piece((keys, values), "sp", 0, 1)
    piece_rows = key_part.shape[0]
    key_block = math.gcd(piece_rows, 1024)

    def attend_piece(running):

        def key_step(block_index, inner_state):
            block_first = block_index * key_block
            key_rows = lax.dynamic_slice_in_dim(key_part, block_first, key_block, 0)
            key_rows = key_rows.reshape(key_block, heads_here, HD).transpose(1, 0, 2)
            value_rows = lax.dynamic_slice_in_dim(value_part, block_first, key_block, 0)
            value_rows = value_rows.reshape(key_block, heads_here, HD).transpose(1, 0, 2)
            cum_keys = lax.dynamic_slice_in_dim(cum_gate, block_first, key_block, 1)
            return attend_block(
                inner_state,
                query_heads,
                cum_query,
                key_rows,
                value_rows,
                cum_keys,
                shift_amount,
                block_first,
            )

        return lax.fori_loop(0, piece_rows // key_block, key_step, running)

    best_score, weight_sum, value_sum = lax.cond(
        jnp.int32(0) <= shift_amount + rows_here - 1,
        attend_piece,
        lambda running: running,
        start_state,
    )
    attended = (value_sum / weight_sum[..., None]).astype(jnp.bfloat16)
    attended = attended.transpose(1, 0, 2).reshape(rows_here, heads_here * HD)
    partial_value = jnp.dot(attended, out_weight, preferred_element_type=jnp.float32)
    mixed_sum = sum_at_owner(partial_value.astype(jnp.bfloat16), "tp", 1)
    stream_cols = (
        lax.dynamic_slice_in_dim(resid, column_first, columns, 1).astype(jnp.float32) + mixed_sum
    )
    square_sum = of_everyone(jnp.sum(stream_cols * stream_cols, axis=1, keepdims=True), "tp")
    gain_cols = lax.dynamic_slice_in_dim(norm_gain, column_first, columns, 0)
    normed = (stream_cols * lax.rsqrt(square_sum / model_width + epsilon) * gain_cols).astype(
        jnp.bfloat16
    )
    capacity = 5 * rows_here // (2 * sp_count)
    chosen = routes.reshape(-1)
    onehot = (chosen[:, None] == jnp.arange(sp_count, dtype=jnp.int32)[None, :]).astype(jnp.int32)
    before = jnp.cumsum(onehot, axis=0) - onehot
    rank_within = jnp.sum(before * onehot, axis=1)
    slot_index = chosen * capacity + rank_within
    source_row = (
        jnp.zeros((sp_count * capacity,), jnp.int32)
        .at[slot_index]
        .set(jnp.arange(chosen.shape[0], dtype=jnp.int32) // routes.shape[1])
    )
    filled = jnp.zeros((sp_count * capacity,), jnp.bool_).at[slot_index].set(True)
    outgoing = jnp.where(filled[:, None], normed[source_row], jnp.zeros((), jnp.bfloat16))
    outgoing = outgoing.reshape(sp_count, capacity, normed.shape[1])
    gate_here = gate_weight[0]
    up_here = up_weight[0]
    local_down_weight = down_weight[0]
    arrived = lax.all_to_all(outgoing, "sp", split_axis=0, concat_axis=0, tiled=True)
    arrived_rows = arrived.reshape(-1, columns)
    col_part = lax.all_gather(arrived_rows, "tp", axis=1, tiled=True)
    gate_sum = jnp.dot(col_part, gate_here, preferred_element_type=jnp.float32)
    up_sum = jnp.dot(col_part, up_here, preferred_element_type=jnp.float32)
    slot_shape = arrived.shape
    hidden = (jax.nn.silu(gate_sum) * up_sum).astype(jnp.bfloat16)
    partial_term = jnp.dot(hidden, local_down_weight, preferred_element_type=jnp.float32)
    expert_rows = sum_at_owner(partial_term.astype(jnp.bfloat16), "tp", 1).astype(jnp.bfloat16)
    returned = expert_rows.reshape(slot_shape[0], slot_shape[1], columns)
    returned_back = lax.all_to_all(returned, "sp", split_axis=0, concat_axis=0, tiled=True)
    returned_flat = returned_back.reshape(sp_count * capacity, columns)
    picked = (
        returned_flat[slot_index].reshape(rows_here, routes.shape[1], columns).astype(jnp.float32)
    )
    combined = jnp.sum(picked * route_weight[..., None], axis=1)
    return (stream_cols + combined).astype(jnp.bfloat16)


def solution(mesh):
    return jax.shard_map(
        local,
        mesh=mesh,
        in_specs=(
            P("sp", "tp"),
            P("sp", "tp"),
            P("sp", "tp"),
            P("tp", None),
            P("tp", None),
            P("sp", None),
            P(),
            P("sp", None),
            P("sp", None),
            P("sp", None, "tp"),
            P("sp", None, "tp"),
            P("sp", "tp", None),
        ),
        out_specs=P("sp", "tp"),
        check_vma=False,
    )
```

profile of v0, /device:TPU:1, one launch (start us, length us, event | category | flops | bytes accessed | tf_op | source)
XLA Modules:
  0.0 370.9 jit_solution(9054272636798588638)
XLA Ops:
  9.1 86.0 %all-gather.3.cloned.1.call-done = bf16[8192,128]{1,0:T(8,128)(2,1)} async-done(((bf16[256,128]{1,0:T(8,128)(2,1)}), bf16[8192,128]{1,0:T(8,128)(2,1)}) %all-gather.3.cloned.1.call-update) | async-done | bytes 2097168 | tf_op jit(solution)/shard_map/all_gather | solution.py:17
  95.1 49.2 %conditional.1 = (f32[1,256]{1,0:T(1,128)}, f32[1,256,64]{1,2,0:T(8,128)}) conditional(s32[]{:T(128)} %convert_element_type.51, () %tuple.31, (bf16[8192,128]{1,0:T(8,128)(2,1)}, bf16[256,64]{0,1:T(8,128)(2,1)}, s32[]{:T(128)}, f32[1,8192]{1,0:T(1,128)}) %tuple.32), branch_computations={%region_0.0_spmd, %region_1.6_spmd} | conditional | flops 70830592 | bytes 8277405 | solution.py:121
  95.9 5.0 %fusion.45 = (bf16[8192,64]{1,0:T(8,128)(2,1)}, bf16[8192,64]{1,0:T(8,128)(2,1)}) fusion(bf16[8192,128]{1,0:T(8,128)(2,1)} %get-tuple-element.217), kind=kLoop, calls=%fused_computation.87 | loop fusion | bytes 4194304 | tf_op jit(solution)/shard_map/split | solution.py:17
  101.0 43.3 %while.20 = (s32[]{:T(128)}, f32[1,256]{1,0:T(1,128)S(1)}, f32[1,256]{1,0:T(1,128)}, f32[1,256,64]{1,2,0:T(8,128)}, s32[]{:T(128)}, /*index=5*/bf16[8192,64]{1,0...) while((s32[]{:T(128)}, f32[1,256]{1,0:T(1,128)S(1)}, ...), condition=%wide.region_5.5_spmd.clone, body=%wide.region_2.4_spmd.clone.sunk | while | flops 70830592 | bytes 3884243 | solution.py:119
  103.9 2.0 fusion.62
  109.3 2.0 fusion.62
  112.1 1.4 fusion.58
  114.8 2.0 fusion.62
  117.6 1.4 fusion.58
  120.3 2.0 fusion.62
  125.8 2.0 fusion.62
  131.3 2.0 fusion.62
  134.0 1.4 fusion.58
  136.8 2.0 fusion.62
  142.2 2.0 fusion.62
  146.8 12.3 %all-to-all-start = ((bf16[16,256,128]{2,1,0:T(8,128)(2,1)}), bf16[16,256,128]{2,1,0:T(8,128)(2,1)S(1)}, u32[]{:S(2)}, u32[]{:S(2)}) async-start(bf16[16,256,128]{2,1,0:T(8,128)(2,1)} %bitcast.74), calls=%async_computation | async-start | bytes 2097152 | tf_op jit(solution)/shard_map/all_to_all | solution.py:27
  161.5 2.4 scatter_custom_fusion.1
  164.0 23.2 %all-to-all-done = bf16[16,256,128]{2,1,0:T(8,128)(2,1)S(1)} async-done(((bf16[16,256,128]{2,1,0:T(8,128)(2,1)}), bf16[16,256,128]{2,1,0:T(8,128)(2,1)S(1)}, u32[]{:S(2)}, u32[]{:S(2)}) %all-to-all-start) | async-done | bytes 1048608 | tf_op jit(solution)/shard_map/all_to_all | solution.py:27
  188.9 3.4 all-to-all-start.1
  193.2 2.4 scatter_custom_fusion
  195.7 3.9 %all-to-all-done.1 = f32[16,256,1]{1,2,0:T(1,128)S(1)} async-done(((f32[16,256,1]{1,2,0:T(1,128)}), f32[16,256,1]{1,2,0:T(1,128)S(1)}, u32[]{:S(2)}, u32[]{:S(2)}) %all-to-all-start.1) | async-done | bytes 16416 | tf_op jit(solution)/shard_map/all_to_all | solution.py:33
  200.7 2.0 gather_fusion
  202.9 15.5 %all_to_all.25 = bf16[32,20,128]{2,1,0:T(8,128)(2,1)S(1)} all-to-all(bf16[32,20,128]{2,1,0:T(8,128)(2,1)S(1)} %broadcast_select_fusion.2), channel_id=1, replica_groups=mesh['sp'=32,'tp'=16] {'sp'}, dimensions={0} | all-to-all | bytes 327680 | tf_op jit(solution)/shard_map/all_to_all | solution.py:156
  219.1 38.1 %all-gather.5.cloned.1.call-done = bf16[640,2048]{1,0:T(8,128)(2,1)} async-done(((bf16[640,128]{1,0:T(8,128)(2,1)}), bf16[640,2048]{1,0:T(8,128)(2,1)}) %all-gather.5.cloned.1.call-update) | async-done | bytes 2621456 | tf_op jit(solution)/shard_map/all_gather | solution.py:158
  257.2 3.4 fusion.26
  260.7 6.2 %fusion.21 = bf16[80,16,8,128]{3,2,1,0:T(8,128)(2,1)} fusion(bf16[1,256,2048]{2,1,0:T(8,128)(2,1)S(1)} %copy-done, bf16[640,2048]{1,0:T(8,128)(2,1)} %all-gather.5.cloned.1.call-done, bf16[1,2048,256]{2,1,0:T(8,128)(2,1)S(1)} %copy-done.6, f32[640,256]{1,0:T(8,128)} %fusion.26), kind=kOutput, calls=%fused_computation.40 | convolution fusion | flops 1344471040 | bytes 7995392 | tf_op jit(solution)/shard_map/dot_general | solution.py:163
  266.9 2.4 copy.43
  269.3 67.0 %all_to_all.26 = bf16[16,640,128]{2,1,0:T(8,128)(2,1)} all-to-all(bf16[16,640,128]{2,1,0:T(8,128)(2,1)S(1)} %bitcast.91), channel_id=1, replica_groups=mesh['sp'=32,'tp'=16] {'tp'}, dimensions={0} | all-to-all | bytes 5242880 | tf_op jit(solution)/shard_map/all_to_all | solution.py:27
  336.3 2.1 reduce_sum.77
  339.2 9.9 %all-to-all-start.4 = ((bf16[32,20,128]{2,1,0:T(8,128)(2,1)}), bf16[32,20,128]{2,1,0:T(8,128)(2,1)S(1)}, u32[]{:S(2)}, u32[]{:S(2)}) async-start(bf16[32,20,128]{2,1,0:T(8,128)(2,1)} %reshape.156), calls=%async_computation.4 | async-start | bytes 393216 | tf_op jit(solution)/shard_map/all_to_all | solution.py:166
  349.3 11.5 %all-to-all-done.4 = bf16[32,20,128]{2,1,0:T(8,128)(2,1)S(1)} async-done(((bf16[32,20,128]{2,1,0:T(8,128)(2,1)}), bf16[32,20,128]{2,1,0:T(8,128)(2,1)S(1)}, u32[]{:S(2)}, u32[]{:S(2)}) %all-to-all-start.4) | async-done | bytes 163872 | tf_op jit(solution)/shard_map/all_to_all | solution.py:166
  362.5 1.5 add_convert_fusion
  (123 shorter events, 38.4 us)
Async XLA Ops:
  6.5 254.1 %copy-start = (bf16[1,256,2048]{2,1,0:T(8,128)(2,1)S(1)}, bf16[1,256,2048]{2,1,0:T(8,128)(2,1)}, u32[]{:S(2)}) copy-start(bf16[1,256,2048]{2,1,0:T(8,128)(2,1)} %param.27) | copy-start | bytes 3145732
  6.5 88.6 %all-gather.3.cloned.1.call-start = ((), (), s32[]{:S(2)}) async-start(), calls=%async_computation.5 | async-start | bytes 2162688 | tf_op jit(solution)/shard_map/all_gather | solution.py:17
  95.1 49.2 %copy-start.1 = (bf16[64,2048]{1,0:T(8,128)(2,1)S(1)}, bf16[64,2048]{1,0:T(8,128)(2,1)}, u32[]{:S(2)}) copy-start(bf16[64,2048]{1,0:T(8,128)(2,1)} %param.20) | copy-start | bytes 786436
  95.9 5.0 %copy-start.2 = (bf16[256,64]{0,1:T(8,128)(2,1)S(1)}, bf16[256,64]{0,1:T(8,128)(2,1)}, u32[]{:S(2)}) copy-start(bf16[256,64]{0,1:T(8,128)(2,1)} %get-tuple-element.272) | copy-start | bytes 98308 | tf_op jit(solution)/shard_map/cond
  144.3 14.9 %copy-start.3 = (s32[256,2]{0,1:T(2,128)S(1)}, s32[256,2]{0,1:T(2,128)}, u32[]{:S(2)}) copy-start(s32[256,2]{0,1:T(2,128)} %param.23) | copy-start | bytes 6148
  146.8 40.3 %all-to-all-start = ((bf16[16,256,128]{2,1,0:T(8,128)(2,1)}), bf16[16,256,128]{2,1,0:T(8,128)(2,1)S(1)}, u32[]{:S(2)}, u32[]{:S(2)}) async-start(bf16[16,256,128]{2,1,0:T(8,128)(2,1)} %bitcast.74), calls=%async_computation | async-start | bytes 2097152 | tf_op jit(solution)/shard_map/all_to_all | solution.py:27
  161.1 96.1 %copy-start.5 = (bf16[1,2048,256]{2,1,0:T(8,128)(2,1)S(1)}, bf16[1,2048,256]{2,1,0:T(8,128)(2,1)}, u32[]{:S(2)}) copy-start(bf16[1,2048,256]{2,1,0:T(8,128)(2,1)} %param.25) | copy-start | bytes 3145732
  188.9 10.8 %all-to-all-start.1 = ((f32[16,256,1]{1,2,0:T(1,128)}), f32[16,256,1]{1,2,0:T(1,128)S(1)}, u32[]{:S(2)}, u32[]{:S(2)}) async-start(f32[16,256,1]{1,2,0:T(1,128)} %broadcast_in_dim.90), calls=%async_computation.1 | async-start | bytes 32768 | tf_op jit(solution)/shard_map/all_to_all | solution.py:33
  192.3 64.9 %all-gather.5.cloned.1.call-start = ((), (), s32[]{:S(2)}) async-start(), calls=%async_computation.6 | async-start | bytes 2785280 | tf_op jit(solution)/shard_map/all_gather | solution.py:158
  219.1 41.5 %copy-start.6 = (bf16[1,2048,256]{2,1,0:T(8,128)(2,1)S(1)}, bf16[1,2048,256]{2,1,0:T(8,128)(2,1)}, u32[]{:S(2)}) copy-start(bf16[1,2048,256]{2,1,0:T(8,128)(2,1)} %param.26) | copy-start | bytes 3145732
  336.3 12.8 %copy-start.4 = (f32[256,2]{0,1:T(2,128)S(1)}, f32[256,2]{0,1:T(2,128)}, u32[]{:S(2)}) copy-start(f32[256,2]{0,1:T(2,128)} %param.24) | copy-start | bytes 6148
  339.2 21.5 %all-to-all-start.4 = ((bf16[32,20,128]{2,1,0:T(8,128)(2,1)}), bf16[32,20,128]{2,1,0:T(8,128)(2,1)S(1)}, u32[]{:S(2)}, u32[]{:S(2)}) async-start(bf16[32,20,128]{2,1,0:T(8,128)(2,1)} %reshape.156), calls=%async_computation.4 | async-start | bytes 393216 | tf_op jit(solution)/shard_map/all_to_all | solution.py:166
Sparse Core Ops, SparseCore 0:
  10.5 84.5 all-gather.2
  219.2 37.9 all-gather.4
where the time goes:
time: 372 us; the launch traced here: 371 us
  waiting for transfers between devices  163 us (44%)
  blocking collectives  82.6 us (22%)
  matrix products  38 us (10%)
  local copies, waits for them, and re-layouts  29.2 us (8%)
  starting transfers between devices  25.7 us (7%)
  other arithmetic  19 us (5%)
  between operations  13.6 us (4%)
    all_gather x1, waiting for transfers between devices, in_one_piece(): lax.all_gather(both, axis, axis=dim, tiled=True)  86 us
    all_to_all x1, blocking collectives, sum_at_owner(): lax.all_to_all(tiles, axis, split_axis=0, concat_axis=0, tiled=True)  67 us
    all_gather x1, waiting for transfers between devices, local(): col_part = lax.all_gather(arrived_rows, 'tp', axis=1, tiled=True)  38.1 us
    all_to_all x1, waiting for transfers between devices, sum_at_owner(): lax.all_to_all(tiles, axis, split_axis=0, concat_axis=0, tiled=True)  23.2 us
    dot_general x8, matrix products, attend_block(): jnp.einsum('hqk,hkd->hqd', weights.astype(jnp.bfloat16), value_rows, pref...  16.2 us
    all_to_all x1, blocking collectives, local(): lax.all_to_all(outgoing, 'sp', split_axis=0, concat_axis=0, tiled=True)  15.5 us
    all_to_all x1, starting transfers between devices, sum_at_owner(): lax.all_to_all(tiles, axis, split_axis=0, concat_axis=0, tiled=True)  12.3 us
    all_to_all x1, waiting for transfers between devices, local(): lax.all_to_all(returned, 'sp', split_axis=0, concat_axis=0, tiled=True)  11.5 us
  transfers between devices with their start and end apart: 5, of which 5 were waited for; matrix products, arithmetic and copies ran while one was open for 2% of the time, Pallas kernels for 0%

commit v1 on v0

--- a/solution.py
+++ b/solution.py
@@ -155,7 +155,9 @@
     local_down_weight = down_weight[0]
     arrived = lax.all_to_all(outgoing, "sp", split_axis=0, concat_axis=0, tiled=True)
     arrived_rows = arrived.reshape(-1, columns)
-    col_part = lax.all_gather(arrived_rows, "tp", axis=1, tiled=True)
+    col_part = jnp.concatenate(
+        lax.all_to_all(jnp.stack([arrived_rows] * lax.axis_size("tp")), "tp", 0, 0), axis=1
+    )
     gate_sum = jnp.dot(col_part, gate_here, preferred_element_type=jnp.float32)
     up_sum = jnp.dot(col_part, up_here, preferred_element_type=jnp.float32)
     slot_shape = arrived.shape

time: 372 us -> 392 us (1.054)
  blocking collectives: 82.6 us -> 147 us
  waiting for transfers between devices: 163 us -> 125 us
  starting transfers between devices: 25.7 us -> 19.6 us
    all_to_all x0 -> x1, blocking collectives: none -> 66.9 us  [local(): lax.all_to_all(jnp.stack([arrived_rows] * lax.axis_size('tp')), 'tp', 0, 0)]
    all_gather x1 -> x0, waiting for transfers between devices: 38.1 us -> none  [local(): col_part = lax.all_gather(arrived_rows, 'tp', axis=1, tiled=True)]
    all_to_all x1, starting transfers between devices: 9.9 us -> 3.87 us  [local(): lax.all_to_all(returned, 'sp', split_axis=0, concat_axis=0, tiled=True)]
  transfers between devices with their start and end apart: 5 -> 4, of which waited for: 5 -> 4; matrix products, arithmetic and copies ran while one was open for 2% -> 2% of each run, Pallas kernels for 0% -> 0%
where the time goes in v1:
time: 392 us; the launch traced here: 390 us
  blocking collectives  147 us (38%)
  waiting for transfers between devices  125 us (32%)
  matrix products  35.3 us (9%)
  local copies, waits for them, and re-layouts  30.8 us (8%)
  starting transfers between devices  19.6 us (5%)
  other arithmetic  19 us (5%)
  between operations  13.6 us (3%)
    all_gather x1, waiting for transfers between devices, in_one_piece(): lax.all_gather(both, axis, axis=dim, tiled=True)  86 us
    all_to_all x1, blocking collectives, local(): lax.all_to_all(jnp.stack([arrived_rows] * lax.axis_size('tp')), 'tp', 0, 0)  66.9 us
    all_to_all x1, blocking collectives, sum_at_owner(): lax.all_to_all(tiles, axis, split_axis=0, concat_axis=0, tiled=True)  64.9 us
    all_to_all x1, waiting for transfers between devices, sum_at_owner(): lax.all_to_all(tiles, axis, split_axis=0, concat_axis=0, tiled=True)  23.2 us
    dot_general x8, matrix products, attend_block(): jnp.einsum('hqk,hkd->hqd', weights.astype(jnp.bfloat16), value_rows, pref...  16.2 us
    all_to_all x1, blocking collectives, local(): lax.all_to_all(outgoing, 'sp', split_axis=0, concat_axis=0, tiled=True)  15.5 us
    all_to_all x1, starting transfers between devices, sum_at_owner(): lax.all_to_all(tiles, axis, split_axis=0, concat_axis=0, tiled=True)  12.3 us
    all_to_all x1, waiting for transfers between devices, local(): lax.all_to_all(returned, 'sp', split_axis=0, concat_axis=0, tiled=True)  11.3 us
  transfers between devices with their start and end apart: 4, of which 4 were waited for; matrix products, arithmetic and copies ran while one was open for 2% of the time, Pallas kernels for 0%

profile of v1, /device:TPU:1, one launch (start us, length us, event | category | flops | bytes accessed | tf_op | source)
XLA Modules:
  0.0 390.4 jit_solution(9431400826930052654)
XLA Ops:
  9.1 86.0 %all-gather.2.cloned.1.call-done = bf16[8192,128]{1,0:T(8,128)(2,1)} async-done(((bf16[256,128]{1,0:T(8,128)(2,1)}), bf16[8192,128]{1,0:T(8,128)(2,1)}) %all-gather.2.cloned.1.call-update) | async-done | bytes 2097168 | tf_op jit(solution)/shard_map/all_gather | solution.py:17
  95.1 49.2 %conditional.1 = (f32[1,256]{1,0:T(1,128)}, f32[1,256,64]{1,2,0:T(8,128)}) conditional(s32[]{:T(128)} %convert_element_type.51, () %tuple.31, (bf16[8192,128]{1,0:T(8,128)(2,1)}, bf16[256,64]{0,1:T(8,128)(2,1)}, s32[]{:T(128)}, f32[1,8192]{1,0:T(1,128)}) %tuple.32), branch_computations={%region_0.0_spmd, %region_1.6_spmd} | conditional | flops 70830592 | bytes 8277405 | solution.py:121
  95.9 5.0 %fusion.45 = (bf16[8192,64]{1,0:T(8,128)(2,1)}, bf16[8192,64]{1,0:T(8,128)(2,1)}) fusion(bf16[8192,128]{1,0:T(8,128)(2,1)} %get-tuple-element.217), kind=kLoop, calls=%fused_computation.87 | loop fusion | bytes 4194304 | tf_op jit(solution)/shard_map/split | solution.py:17
  101.0 43.3 %while.20 = (s32[]{:T(128)}, f32[1,256]{1,0:T(1,128)S(1)}, f32[1,256]{1,0:T(1,128)}, f32[1,256,64]{1,2,0:T(8,128)}, s32[]{:T(128)}, /*index=5*/bf16[8192,64]{1,0...) while((s32[]{:T(128)}, f32[1,256]{1,0:T(1,128)S(1)}, ...), condition=%wide.region_5.5_spmd.clone, body=%wide.region_2.4_spmd.clone.sunk | while | flops 70830592 | bytes 3884243 | solution.py:119
  103.9 2.0 fusion.62
  109.3 2.0 fusion.62
  112.1 1.4 fusion.58
  114.8 2.0 fusion.62
  117.6 1.4 fusion.58
  120.3 2.0 fusion.62
  125.8 2.0 fusion.62
  131.3 2.0 fusion.62
  134.0 1.4 fusion.58
  136.8 2.0 fusion.62
  142.2 2.0 fusion.62
  146.8 12.3 %all-to-all-start = ((bf16[16,256,128]{2,1,0:T(8,128)(2,1)}), bf16[16,256,128]{2,1,0:T(8,128)(2,1)S(1)}, u32[]{:S(2)}, u32[]{:S(2)}) async-start(bf16[16,256,128]{2,1,0:T(8,128)(2,1)} %bitcast.77), calls=%async_computation | async-start | bytes 2097152 | tf_op jit(solution)/shard_map/all_to_all | solution.py:27
  161.5 2.4 scatter_custom_fusion.1
  164.0 23.2 %all-to-all-done = bf16[16,256,128]{2,1,0:T(8,128)(2,1)S(1)} async-done(((bf16[16,256,128]{2,1,0:T(8,128)(2,1)}), bf16[16,256,128]{2,1,0:T(8,128)(2,1)S(1)}, u32[]{:S(2)}, u32[]{:S(2)}) %all-to-all-start) | async-done | bytes 1048608 | tf_op jit(solution)/shard_map/all_to_all | solution.py:27
  188.9 3.4 all-to-all-start.1
  193.1 2.4 scatter_custom_fusion
  195.7 4.0 %all-to-all-done.1 = f32[16,256,1]{1,2,0:T(1,128)S(1)} async-done(((f32[16,256,1]{1,2,0:T(1,128)}), f32[16,256,1]{1,2,0:T(1,128)S(1)}, u32[]{:S(2)}, u32[]{:S(2)}) %all-to-all-start.1) | async-done | bytes 16416 | tf_op jit(solution)/shard_map/all_to_all | solution.py:33
  200.7 2.0 gather_fusion
  202.9 15.5 %all_to_all.30 = bf16[32,20,128]{2,1,0:T(8,128)(2,1)S(1)} all-to-all(bf16[32,20,128]{2,1,0:T(8,128)(2,1)S(1)} %broadcast_select_fusion.2), channel_id=1, replica_groups=mesh['sp'=32,'tp'=16] {'sp'}, dimensions={0} | all-to-all | bytes 327680 | tf_op jit(solution)/shard_map/all_to_all | solution.py:156
  218.9 66.9 %all_to_all.31 = bf16[16,640,128]{1,2,0:T(8,128)(2,1)S(1)} all-to-all(bf16[16,640,128]{1,2,0:T(8,128)(2,1)S(1)} %stack.3), channel_id=1, replica_groups=mesh['sp'=32,'tp'=16] {'tp'}, dimensions={0} | all-to-all | bytes 5242880 | tf_op jit(solution)/shard_map/all_to_all | solution.py:159
  285.9 1.5 copy-done.1
  288.6 6.1 %fusion.21 = bf16[80,16,8,128]{3,2,1,0:T(8,128)(2,1)} fusion(bf16[1,256,2048]{2,1,0:T(8,128)(2,1)S(1)} %copy-done, bf16[640,2048]{0,1:T(8,128)(2,1)} %bitcast.96, bf16[1,2048,256]{2,1,0:T(8,128)(2,1)S(1)} %copy-done.7, f32[640,256]{1,0:T(8,128)S(1)} %fusion.26), kind=kOutput, calls=%fused_computation.40 | convolution fusion | flops 1344471040 | bytes 7995392 | tf_op jit(solution)/shard_map/dot_general | solution.py:165
  294.7 2.4 copy.45
  297.1 64.9 %all_to_all.32 = bf16[16,640,128]{2,1,0:T(8,128)(2,1)} all-to-all(bf16[16,640,128]{2,1,0:T(8,128)(2,1)S(1)} %bitcast.94), channel_id=1, replica_groups=mesh['sp'=32,'tp'=16] {'tp'}, dimensions={0} | all-to-all | bytes 5242880 | tf_op jit(solution)/shard_map/all_to_all | solution.py:27
  362.1 2.1 reduce_sum.77
  364.9 3.9 all-to-all-start.5
  368.9 11.3 %all-to-all-done.5 = bf16[32,20,128]{2,1,0:T(8,128)(2,1)S(1)} async-done(((bf16[32,20,128]{2,1,0:T(8,128)(2,1)}), bf16[32,20,128]{2,1,0:T(8,128)(2,1)S(1)}, u32[]{:S(2)}, u32[]{:S(2)}) %all-to-all-start.5) | async-done | bytes 163872 | tf_op jit(solution)/shard_map/all_to_all | solution.py:168
  382.1 1.5 add_convert_fusion
  (125 shorter events, 39.4 us)
Async XLA Ops:
  6.5 281.7 %copy-start = (bf16[1,256,2048]{2,1,0:T(8,128)(2,1)S(1)}, bf16[1,256,2048]{2,1,0:T(8,128)(2,1)}, u32[]{:S(2)}) copy-start(bf16[1,256,2048]{2,1,0:T(8,128)(2,1)} %param.27) | copy-start | bytes 3145732
  6.5 88.6 %all-gather.2.cloned.1.call-start = ((), (), s32[]{:S(2)}) async-start(), calls=%async_computation.6 | async-start | bytes 2162688 | tf_op jit(solution)/shard_map/all_gather | solution.py:17
  95.1 49.2 %copy-start.2 = (bf16[64,2048]{1,0:T(8,128)(2,1)S(1)}, bf16[64,2048]{1,0:T(8,128)(2,1)}, u32[]{:S(2)}) copy-start(bf16[64,2048]{1,0:T(8,128)(2,1)} %param.20) | copy-start | bytes 786436
  95.9 5.0 %copy-start.3 = (bf16[256,64]{0,1:T(8,128)(2,1)S(1)}, bf16[256,64]{0,1:T(8,128)(2,1)}, u32[]{:S(2)}) copy-start(bf16[256,64]{0,1:T(8,128)(2,1)} %get-tuple-element.272) | copy-start | bytes 98308 | tf_op jit(solution)/shard_map/cond
  144.3 14.9 %copy-start.4 = (s32[256,2]{0,1:T(2,128)S(1)}, s32[256,2]{0,1:T(2,128)}, u32[]{:S(2)}) copy-start(s32[256,2]{0,1:T(2,128)} %param.23) | copy-start | bytes 6148
  146.8 40.3 %all-to-all-start = ((bf16[16,256,128]{2,1,0:T(8,128)(2,1)}), bf16[16,256,128]{2,1,0:T(8,128)(2,1)S(1)}, u32[]{:S(2)}, u32[]{:S(2)}) async-start(bf16[16,256,128]{2,1,0:T(8,128)(2,1)} %bitcast.77), calls=%async_computation | async-start | bytes 2097152 | tf_op jit(solution)/shard_map/all_to_all | solution.py:27
  188.9 10.8 %all-to-all-start.1 = ((f32[16,256,1]{1,2,0:T(1,128)}), f32[16,256,1]{1,2,0:T(1,128)S(1)}, u32[]{:S(2)}, u32[]{:S(2)}) async-start(f32[16,256,1]{1,2,0:T(1,128)} %broadcast_in_dim.90), calls=%async_computation.1 | async-start | bytes 32768 | tf_op jit(solution)/shard_map/all_to_all | solution.py:33
  218.9 68.4 %copy-start.6 = (bf16[1,2048,256]{2,1,0:T(8,128)(2,1)S(1)}, bf16[1,2048,256]{2,1,0:T(8,128)(2,1)}, u32[]{:S(2)}) copy-start(bf16[1,2048,256]{2,1,0:T(8,128)(2,1)} %param.25) | copy-start | bytes 3145732
  285.9 1.5 copy-start.1
  287.4 1.2 copy-start.7
  362.1 6.7 %copy-start.5 = (f32[256,2]{0,1:T(2,128)S(1)}, f32[256,2]{0,1:T(2,128)}, u32[]{:S(2)}) copy-start(f32[256,2]{0,1:T(2,128)} %param.24) | copy-start | bytes 6148
  364.9 15.4 %all-to-all-start.5 = ((bf16[32,20,128]{2,1,0:T(8,128)(2,1)}), bf16[32,20,128]{2,1,0:T(8,128)(2,1)S(1)}, u32[]{:S(2)}, u32[]{:S(2)}) async-start(bf16[32,20,128]{2,1,0:T(8,128)(2,1)} %reshape.162), calls=%async_computation.5 | async-start | bytes 393216 | tf_op jit(solution)/shard_map/all_to_all | solution.py:168
Sparse Core Ops, SparseCore 0:
  10.5 84.5 all-gather.1
